TPU v7x, 128 devices: a whole 4x4x4 slice. The times are simulated.
128 devices in a mesh: ep: 128 (over z, y, x, core).
Axes of the slice: x: 4, y: 4, z: 4, core: 2. Of those that a mesh axis runs over, the one named last changes fastest.
Arguments:
- tokens: bfloat16 [32768, 2048], P('ep'), may hold values from -6 to 6
- norm_gain: float32 [2048], replicated, may hold values from 0.1 to 1.9
- expert_ids: int32 [32768, 2], P('ep'), may hold values from 0 to 127, as said below
- gates: float32 [32768, 2], P('ep'), may hold values from 0.1 to 1
- w_gate: bfloat16 [128, 2048, 1024], P('ep'), may hold values from -0.125 to 0.125
- w_up: bfloat16 [128, 2048, 1024], P('ep'), may hold values from -0.125 to 0.125
- w_down: bfloat16 [128, 1024, 2048], P('ep'), may hold values from -0.1875 to 0.1875
Outputs:
- combined: bfloat16 [32768, 2048], P('ep')
Inputs may be any that keep to these rules, and one draw needn't show every extreme that they name: `expert_ids`: each row names two different experts of one group, a group being 4 consecutive expert numbers. Among the rows of one device no expert is named more than 8 times, and some expert is named exactly 8 times; some expert is named exactly 8 times by the rows of every device.
All inputs are finite; a program needn't handle non-finite values.
Results may differ from a plain program's by a relative error of at most 0.0085.
Values may be sent and summed in bfloat16 or wider, within the bound.
A program may use at most 128 MiB of HBM per device.

v0:
```python
import jax
import jax.numpy as jnp
from jax import lax
from jax.sharding import PartitionSpec as P

EPS = 1e-06


def normalize(tokens, norm_gain):
    floats = tokens.astype(jnp.float32)
    inverse_rms = lax.rsqrt(jnp.mean(floats * floats, axis=-1, keepdims=True) + EPS)
    return (floats * inverse_rms * norm_gain).astype(jnp.bfloat16)


def expert_rows(block_rows, gate_weight, up_weight, down_weight):
    gate_part = jnp.dot(block_rows, gate_weight, preferred_element_type=jnp.float32)
    up_part = jnp.dot(block_rows, up_weight, preferred_element_type=jnp.float32)
    hidden = (jax.nn.silu(gate_part) * up_part).astype(jnp.bfloat16)
    return jnp.dot(hidden, down_weight, preferred_element_type=jnp.float32).astype(jnp.bfloat16)


def shards(tokens, norm_gain, expert_ids, gates, w_gate, w_up, w_down):
    tok_rows, model_width = tokens.shape
    experts = lax.axis_size("ep")
    capacity = 2 * ((2 * tok_rows + experts - 1) // experts)
    normed = normalize(tokens, norm_gain)
    gate_weight = w_gate[0]
    up_weight = w_up[0]
    down_weight = w_down[0]
    flat_ids = expert_ids.reshape(-1)
    one_hot = (flat_ids[:, None] == jnp.arange(experts, dtype=jnp.int32)[None, :]).astype(jnp.int32)
    earlier = jnp.cumsum(one_hot, axis=0) - one_hot
    slot_index = jnp.sum(earlier * one_hot, axis=1)
    buffer_row = flat_ids * capacity + slot_index
    token_row = jnp.arange(2 * tok_rows, dtype=jnp.int32) // 2
    source_row = jnp.full((experts * capacity,), tok_rows, jnp.int32).at[buffer_row].set(token_row)
    padded = jnp.concatenate([normed, jnp.zeros((1, model_width), jnp.bfloat16)], axis=0)
    outgoing = jnp.take(padded, source_row, axis=0).reshape(experts, capacity, model_width)
    arrived = lax.all_to_all(outgoing, "ep", split_axis=0, concat_axis=0, tiled=True)
    produced = expert_rows(arrived.reshape(-1, model_width), gate_weight, up_weight, down_weight)
    produced = produced.reshape(experts, capacity, model_width)
    returned = lax.all_to_all(produced, "ep", split_axis=0, concat_axis=0, tiled=True)
    results = returned.reshape(experts * capacity, model_width)
    picked = (
        jnp.take(results, buffer_row, axis=0).astype(jnp.float32).reshape(tok_rows, 2, model_width)
    )
    combined = jnp.sum(picked * gates[:, :, None], axis=1)
    return combined.astype(jnp.bfloat16)


def solution(mesh):
    return jax.shard_map(
        shards,
        mesh=mesh,
        in_specs=(
            P("ep", None),
            P(),
            P("ep", None),
            P("ep", None),
            P("ep", None, None),
            P("ep", None, None),
            P("ep", None, None),
        ),
        out_specs=P("ep", None),
        check_vma=False,
    )
```

profile of v0, /device:TPU:1, one launch (start us, length us, event | category | flops | bytes accessed | tf_op | source)
XLA Modules:
  0.0 176.2 jit_solution(5364122500480822570)
XLA Ops:
  0.0 0.9 copy.16
  0.9 0.1 eq.26
  1.1 0.1 reshape.93
  1.2 0.7 broadcast_multiply_fusion
  2.0 0.2 fusion.19
  2.3 0.1 copy.22
  2.5 0.1 mul.59
  2.6 0.2 fusion.18
  2.9 2.4 %scatter_custom_fusion = s32[1024]{0:T(1024)S(1)} fusion(s32[512]{0:T(512)S(1)} %bitcast.45, s32[512]{0:T(512)S(1)} %add_select_fusion, s32[]{:T(128)} %constant.57.clone.1), kind=kCustom, calls=%fused_computation.44 | custom fusion | bytes 4100 | tf_op jit(solution)/shard_map/scatter | solution.py:36
  5.3 1.5 fusion.14
  7.0 1.0 fusion.16
  8.1 6.0 %gather_fusion = bf16[1024,2048]{1,0:T(8,128)(2,1)} fusion(bf16[257,2048]{1,0:T(8,128)(2,1)S(1)} %concatenate.3, s32[1024]{0:T(1024)S(1)} %fusion.22), kind=kCustom, calls=%fused_computation | custom fusion | bytes 8392704 | tf_op jit(solution)/shard_map/jit(_take)/gather | solution.py:38
  14.1 2.6 %bitcast_select_fusion = bf16[128,8,2048]{2,1,0:T(8,128)(2,1)S(1)} fusion(bf16[1024,2048]{1,0:T(8,128)(2,1)} %gather_fusion, pred[128,8]{1,0:T(8,128)(4,1)S(1)} %broadcast_in_dim.35), kind=kLoop, calls=%fused_computation.11 | loop fusion | flops 2097152 | bytes 8389632 | tf_op jit(solution)/shard_map/jit(_take)/select_n | solution.py:38
  16.7 64.2 %all_to_all.10 = bf16[128,8,2048]{2,1,0:T(8,128)(2,1)S(1)} all-to-all(bf16[128,8,2048]{2,1,0:T(8,128)(2,1)S(1)} %bitcast_select_fusion), channel_id=1, replica_groups=mesh['ep'=128] {'ep'}, dimensions={0} | all-to-all | bytes 8388608 | tf_op jit(solution)/shard_map/all_to_all | solution.py:39
  81.0 4.5 %fusion.2 = f32[1024,1024]{1,0:T(8,128)S(1)} fusion(bf16[1,2048,1024]{2,1,0:T(8,128)(2,1)S(1)} %copy-done.3, bf16[128,8,2048]{2,1,0:T(8,128)(2,1)S(1)} %all_to_all.10), kind=kOutput, calls=%fused_computation.5 | convolution fusion | flops 4294967296 | bytes 12582912 | tf_op jit(solution)/shard_map/dot_general | solution.py:17
  85.5 5.4 %multiply_convert_fusion = bf16[1024,1024]{1,0:T(8,128)(2,1)S(1)} fusion(f32[1024,1024]{1,0:T(8,128)S(1)} %fusion.2, bf16[1,2048,1024]{2,1,0:T(8,128)(2,1)S(1)} %copy-done.4, bf16[128,8,2048]{2,1,0:T(8,128)(2,1)S(1)} %all_to_all.10), kind=kOutput, calls=%fused_computation.14 | convolution fusion | flops 4301258752 | bytes 14680064 | tf_op jit(solution)/shard_map/dot_general | solution.py:16
  90.9 6.1 %convert_bitcast_fusion = bf16[128,8,2048]{2,1,0:T(8,128)(2,1)} fusion(bf16[1024,1024]{1,0:T(8,128)(2,1)S(1)} %multiply_convert_fusion, bf16[1,1024,2048]{2,1,0:T(8,128)(2,1)S(1)} %copy-done.5), kind=kOutput, calls=%fused_computation.13 | convolution fusion | flops 4297064448 | bytes 10485760 | tf_op jit(solution)/shard_map/dot_general | solution.py:19
  97.0 5.8 %all-to-all-start.1 = ((bf16[128,8,2048]{2,1,0:T(8,128)(2,1)}), bf16[128,8,2048]{2,1,0:T(8,128)(2,1)}, u32[]{:S(2)}, u32[]{:S(2)}) async-start(bf16[128,8,2048]{2,1,0:T(8,128)(2,1)} %convert_bitcast_fusion), calls=%async_computation.1 | async-start | bytes 8388608 | tf_op jit(solution)/shard_map/all_to_all | solution.py:42
  102.8 0.1 reduce_sum.32
  103.1 0.2 copy.21
  103.4 52.1 %all-to-all-done.1 = bf16[128,8,2048]{2,1,0:T(8,128)(2,1)} async-done(((bf16[128,8,2048]{2,1,0:T(8,128)(2,1)}), bf16[128,8,2048]{2,1,0:T(8,128)(2,1)}, u32[]{:S(2)}, u32[]{:S(2)}) %all-to-all-start.1) | async-done | bytes 4194336 | tf_op jit(solution)/shard_map/all_to_all | solution.py:42
  155.5 7.1 %gather_fusion.1 = bf16[512,2048]{1,0:T(8,128)(2,1)S(1)} fusion(bf16[1024,2048]{1,0:T(8,128)(2,1)} %bitcast.11, s32[1024]{0:T(1024)S(1)} %pad_clamp_fusion), kind=kCustom, calls=%fused_computation.1 | custom fusion | bytes 4196352 | tf_op jit(solution)/shard_map/jit(_take)/gather | solution.py:45
  162.7 2.7 %gather.15 = bf16[256,2,2048]{2,1,0:T(2,128)(2,1)} reshape(bf16[512,2048]{1,0:T(8,128)(2,1)S(1)} %gather_fusion.1) | data formatting | bytes 4194304 | tf_op jit(solution)/shard_map/jit(_take)/gather | solution.py:45
  165.4 10.8 %multiply_reduce_fusion = bf16[256,2048]{1,0:T(8,128)(2,1)} fusion(bf16[256,2,2048]{2,1,0:T(2,128)(2,1)} %gather.15, pred[256,2]{1,0:T(8,128)(4,1)S(1)} %copy.21, f32[256,2]{1,0:T(8,128)S(1)} %copy.23), kind=kLoop, calls=%fused_computation.12 | loop fusion | flops 3670016 | bytes 3148288 | tf_op jit(solution)/shard_map/reduce_sum | solution.py:47
  (30 shorter events, 0.7 us)
Async XLA Ops:
  0.0 7.0 %copy-start = (bf16[256,2048]{1,0:T(8,128)(2,1)S(1)}, bf16[256,2048]{1,0:T(8,128)(2,1)}, u32[]{:S(2)}) copy-start(bf16[256,2048]{1,0:T(8,128)(2,1)} %param.7) | copy-start | bytes 3145732
  16.7 64.2 %copy-start.3 = (bf16[1,2048,1024]{2,1,0:T(8,128)(2,1)S(1)}, bf16[1,2048,1024]{2,1,0:T(8,128)(2,1)}, u32[]{:S(2)}) copy-start(bf16[1,2048,1024]{2,1,0:T(8,128)(2,1)} %param.12) | copy-start | bytes 12582916
  81.0 4.5 %copy-start.4 = (bf16[1,2048,1024]{2,1,0:T(8,128)(2,1)S(1)}, bf16[1,2048,1024]{2,1,0:T(8,128)(2,1)}, u32[]{:S(2)}) copy-start(bf16[1,2048,1024]{2,1,0:T(8,128)(2,1)} %param.11) | copy-start | bytes 12582916
  85.5 5.4 %copy-start.5 = (bf16[1,1024,2048]{2,1,0:T(8,128)(2,1)S(1)}, bf16[1,1024,2048]{2,1,0:T(8,128)(2,1)}, u32[]{:S(2)}) copy-start(bf16[1,1024,2048]{2,1,0:T(8,128)(2,1)} %param.13) | copy-start | bytes 12582916
  97.0 6.1 %copy-start.1 = (s32[256,2]{0,1:T(2,128)S(1)}, s32[256,2]{0,1:T(2,128)}, u32[]{:S(2)}) copy-start(s32[256,2]{0,1:T(2,128)} %param.9) | copy-start | bytes 6148
  97.0 6.3 %copy-start.2 = (f32[256,2]{0,1:T(2,128)S(1)}, f32[256,2]{0,1:T(2,128)}, u32[]{:S(2)}) copy-start(f32[256,2]{0,1:T(2,128)} %param.10) | copy-start | bytes 6148
  97.0 58.5 %all-to-all-start.1 = ((bf16[128,8,2048]{2,1,0:T(8,128)(2,1)}), bf16[128,8,2048]{2,1,0:T(8,128)(2,1)}, u32[]{:S(2)}, u32[]{:S(2)}) async-start(bf16[128,8,2048]{2,1,0:T(8,128)(2,1)} %convert_bitcast_fusion), calls=%async_computation.1 | async-start | bytes 8388608 | tf_op jit(solution)/shard_map/all_to_all | solution.py:42
where the time goes:
time: 177 us; the launch traced here: 176 us
  blocking collectives  64.2 us (36%)
  waiting for transfers between devices  52.1 us (29%)
  local copies, waits for them, and re-layouts  20.6 us (12%)
  other arithmetic  17.2 us (10%)
  matrix products  16 us (9%)
  starting transfers between devices  5.82 us (3%)
    all_to_all x1, blocking collectives, shards(): lax.all_to_all(outgoing, 'ep', split_axis=0, concat_axis=0, tiled=True)  64.2 us
    all_to_all x1, waiting for transfers between devices, shards(): lax.all_to_all(produced, 'ep', split_axis=0, concat_axis=0, tiled=True)  52.1 us
    reduce_sum x1, other arithmetic, shards(): combined = jnp.sum(picked * gates[:, :, None], axis=1)  10.8 us
    gather x2, local copies, waits for them, and re-layouts, shards(): jnp.take(results, buffer_row, axis=0).astype(jnp.float32)  9.8 us
    dot_general x1, matrix products, expert_rows(): jnp.dot(hidden, down_weight, preferred_element_type=jnp.float32)  6.09 us
    gather x1, local copies, waits for them, and re-layouts, shards(): jnp.take(padded, source_row, axis=0).reshape(experts, capacity, model_width)  6.02 us
    all_to_all x1, starting transfers between devices, shards(): lax.all_to_all(produced, 'ep', split_axis=0, concat_axis=0, tiled=True)  5.82 us
    dot_general x1, matrix products, expert_rows(): jnp.dot(block_rows, gate_weight, preferred_element_type=jnp.float32)  5.36 us
  transfers between devices with their start and end apart: 1, of which 1 were waited for; matrix products, arithmetic and copies ran while one was open for 0% of the time, Pallas kernels for 0%

commit v1 on v0

v1 whole, which is shorter than its diff:
```python
import jax
import jax.numpy as jnp
from jax import lax
from jax.experimental import pallas as pl
from jax.experimental.pallas import tpu as pltpu
from jax.sharding import PartitionSpec as P

EPS = 1e-06
F32 = jnp.float32
BF16 = jnp.bfloat16


def iota(shape, dim):
    return lax.broadcasted_iota(jnp.int32, shape, dim)


def ones_where(mask):
    return jnp.where(mask, 1.0, 0.0).astype(BF16)


def dot(a, b):
    return jnp.dot(a, b, preferred_element_type=F32)


def pack_kernel(tokens_ref, gain_ref, ids_ref, out_ref, normed_ref, pick_ref):
    rows, width = tokens_ref.shape
    slots = out_ref.shape[0]
    experts = slots // 8
    floats = tokens_ref[...].astype(F32)
    mean = jnp.sum(floats * floats, axis=1, keepdims=True) * (1.0 / width)
    normed_ref[...] = (floats * lax.rsqrt(mean + EPS) * gain_ref[...]).astype(BF16)
    expert = iota((experts, rows), 0)
    named = (expert == ids_ref[0:1, :]) | (expert == ids_ref[1:2, :])
    before = ones_where(iota((rows, rows), 0) < iota((rows, rows), 1))
    rank = dot(ones_where(named), before)
    rank = jnp.where(named, rank, -1.0).astype(BF16)
    spread = ones_where(iota((slots, experts), 0) // 8 == iota((slots, experts), 1))
    slot = (iota((slots, rows), 0) % 8).astype(F32)
    pick_ref[...] = ones_where(dot(spread, rank) == slot)
    for start in range(0, width, 512):
        columns = pl.ds(start, 512)
        out_ref[:, columns] = dot(pick_ref[...], normed_ref[:, columns]).astype(BF16)


def combine_kernel(results_ref, ids_ref, gates_ref, out_ref, first_ref, second_ref):
    slots, width = results_ref.shape
    rows = out_ref.shape[0]
    experts = slots // 8
    expert = iota((rows, experts), 1)
    first, second = ids_ref[:, 0:1], ids_ref[:, 1:2]
    named = (expert == first) | (expert == second)
    before = ones_where(iota((rows, rows), 1) < iota((rows, rows), 0))
    rank = dot(before, ones_where(named))
    rank = jnp.where(named, rank, -1.0).astype(BF16)
    spread = ones_where(iota((experts, slots), 1) // 8 == iota((experts, slots), 0))
    column = iota((rows, slots), 1)
    held = dot(rank, spread) == (column % 8).astype(F32)
    first_ref[...] = ones_where(held & (column // 8 == first))
    second_ref[...] = ones_where(held & (column // 8 == second))
    for start in range(0, width, 512):
        columns = pl.ds(start, 512)
        picked = results_ref[:, columns]
        total = dot(first_ref[...], picked) * gates_ref[:, 0:1] + dot(second_ref[...], picked) * gates_ref[:, 1:2]
        out_ref[:, columns] = total.astype(BF16)


def whole():
    return pl.BlockSpec(memory_space=pltpu.VMEM)


def shards(tokens, norm_gain, expert_ids, gates, w_gate, w_up, w_down):
    rows, width = tokens.shape
    experts = lax.axis_size("ep")
    slots = experts * 8
    outgoing = pl.pallas_call(
        pack_kernel,
        out_shape=jax.ShapeDtypeStruct((slots, width), BF16),
        in_specs=[whole()] * 3,
        out_specs=whole(),
        scratch_shapes=[pltpu.VMEM((rows, width), BF16), pltpu.VMEM((slots, rows), BF16)],
        compiler_params=pltpu.CompilerParams(vmem_limit_bytes=40 << 20),
        name="pack",
    )(tokens, norm_gain.reshape(1, width), expert_ids.T)
    arrived = lax.all_to_all(outgoing.reshape(experts, 8, width), "ep", split_axis=0, concat_axis=0, tiled=True)
    block_rows = arrived.reshape(slots, width)
    gate_part = dot(block_rows, w_gate[0])
    up_part = dot(block_rows, w_up[0])
    hidden = (jax.nn.silu(gate_part) * up_part).astype(BF16)
    produced = dot(hidden, w_down[0]).astype(BF16)
    returned = lax.all_to_all(produced.reshape(experts, 8, width), "ep", split_axis=0, concat_axis=0, tiled=True)
    return pl.pallas_call(
        combine_kernel,
        out_shape=jax.ShapeDtypeStruct((rows, width), BF16),
        in_specs=[whole()] * 3,
        out_specs=whole(),
        scratch_shapes=[pltpu.VMEM((rows, slots), BF16)] * 2,
        compiler_params=pltpu.CompilerParams(vmem_limit_bytes=40 << 20),
        name="combine",
    )(returned.reshape(slots, width), expert_ids, gates)


def solution(mesh):
    return jax.shard_map(
        shards,
        mesh=mesh,
        in_specs=(
            P("ep", None),
            P(),
            P("ep", None),
            P("ep", None),
            P("ep", None, None),
            P("ep", None, None),
            P("ep", None, None),
        ),
        out_specs=P("ep", None),
        check_vma=False,
    )
```

time: 177 us -> 149 us (0.84)
  local copies, waits for them, and re-layouts: 20.6 us -> 2.89 us
  other arithmetic: 17.2 us -> 0 us
  Pallas kernels: 0 us -> 7.64 us
    gather x3 -> x0, local copies, waits for them, and re-layouts: 15.8 us -> none  [the longest x2 9.8 us: shards(): jnp.take(results, buffer_row, axis=0).astype(jnp.float32)]
    reduce_sum x3 -> x0, other arithmetic: 12.6 us -> none  [the longest x1 10.8 us: shards(): combined = jnp.sum(picked * gates[:, :, None], axis=1)]
    pallas_call x0 -> x2, Pallas kernels: none -> 7.64 us  [the longest x1 5.94 us: shards(): pl.pallas_call(combine_kernel, out_shape=jax.ShapeDtypeStruct((rows, widt...]
    select_n x3 -> x0, other arithmetic: 2.65 us -> none  [the longest x1 2.64 us: shards(): jnp.take(padded, source_row, axis=0).reshape(experts, capacity, model_width)]
    scatter x1 -> x0, local copies, waits for them, and re-layouts: 2.45 us -> none  [shards(): jnp.full((experts * capacity,), tok_rows, jnp.int32).at[buffer_row]]
    unnamed x15 -> x18, local copies, waits for them, and re-layouts: 1.06 us -> 2.89 us
where the time goes in v1:
time: 149 us
  blocking collectives  64.2 us (43%)
  waiting for transfers between devices  52.4 us (35%)
  matrix products  15.9 us (11%)
  Pallas kernels  7.64 us (5%)
  starting transfers between devices  5.65 us (4%)
  local copies, waits for them, and re-layouts  2.89 us (2%)
    all_to_all x1, blocking collectives, shards(): lax.all_to_all(outgoing.reshape(experts, 8, width), 'ep', split_axis=0, c...  64.2 us
    all_to_all x1, waiting for transfers between devices, shards(): lax.all_to_all(produced.reshape(experts, 8, width), 'ep', split_axis=0, c...  52.4 us
    dot_general x3, matrix products, dot(): return jnp.dot(a, b, preferred_element_type=F32)  15.9 us
    pallas_call x1, Pallas kernels, shards(): pl.pallas_call(combine_kernel, out_shape=jax.ShapeDtypeStruct((rows, widt...  5.94 us
    all_to_all x1, starting transfers between devices, shards(): lax.all_to_all(produced.reshape(experts, 8, width), 'ep', split_axis=0, c...  5.65 us
  transfers between devices with their start and end apart: 1, of which 1 were waited for; matrix products, arithmetic and copies ran while one was open for 0% of the time, Pallas kernels for 0%

profile of v1, /device:TPU:1, one launch (start us, length us, event | category | flops | bytes accessed | tf_op | source)
XLA Modules:
  0.0 148.9 jit_solution(18362738090473238448)
XLA Ops:
  0.0 0.0 copy-start
  0.0 1.2 copy-done
  1.2 0.0 copy-start.1
  1.2 0.7 copy-done.1
  1.9 0.0 copy-start.2
  1.9 0.7 copy-done.2
  2.6 1.7 %pack.1 = bf16[1024,2048]{1,0:T(8,128)(2,1)S(1)} custom-call(bf16[256,2048]{1,0:T(8,128)(2,1)S(1)} %copy-done, f32[1,2048]{1,0:T(1,128)S(1)} %bitcast.28, s32[2,256]{1,0:T(2,128)S(1)} %bitcast.29), custom_call_target="tpu_custom_call" | custom-call | tf_op jit(solution)/shard_map/pack/pallas_call | solution.py:75
  4.3 0.0 copy-start.5
  4.3 64.2 %all_to_all.10 = bf16[128,8,2048]{2,1,0:T(8,128)(2,1)S(1)} all-to-all(bf16[128,8,2048]{2,1,0:T(8,128)(2,1)S(1)} %bitcast.27), channel_id=1, replica_groups=mesh['ep'=128] {'ep'}, dimensions={0} | all-to-all | bytes 8388608 | tf_op jit(solution)/shard_map/all_to_all | solution.py:84
  68.6 0.0 copy-done.5
  68.6 0.0 copy-start.6
  68.6 4.5 %fusion.2 = f32[1024,1024]{1,0:T(8,128)S(1)} fusion(bf16[1,2048,1024]{2,1,0:T(8,128)(2,1)S(1)} %copy-done.5, bf16[128,8,2048]{2,1,0:T(8,128)(2,1)S(1)} %all_to_all.10), kind=kOutput, calls=%fused_computation.2 | convolution fusion | flops 4294967296 | bytes 12582912 | tf_op jit(solution)/shard_map/dot_general | solution.py:22
  73.1 0.0 copy-done.6
  73.1 0.0 copy-start.7
  73.1 5.4 %multiply_convert_fusion = bf16[1024,1024]{1,0:T(8,128)(2,1)S(1)} fusion(f32[1024,1024]{1,0:T(8,128)S(1)} %fusion.2, bf16[1,2048,1024]{2,1,0:T(8,128)(2,1)S(1)} %copy-done.6, bf16[128,8,2048]{2,1,0:T(8,128)(2,1)S(1)} %all_to_all.10), kind=kOutput, calls=%fused_computation.9 | convolution fusion | flops 4301258752 | bytes 14680064 | tf_op jit(solution)/shard_map/dot_general | solution.py:22
  78.4 0.0 copy-done.7
  78.4 6.1 %convert_bitcast_fusion = bf16[128,8,2048]{2,1,0:T(8,128)(2,1)} fusion(bf16[1024,1024]{1,0:T(8,128)(2,1)S(1)} %multiply_convert_fusion, bf16[1,1024,2048]{2,1,0:T(8,128)(2,1)S(1)} %copy-done.7), kind=kOutput, calls=%fused_computation.8 | convolution fusion | flops 4297064448 | bytes 10485760 | tf_op jit(solution)/shard_map/dot_general | solution.py:22
  84.5 5.7 %all-to-all-start.1 = ((bf16[128,8,2048]{2,1,0:T(8,128)(2,1)}), bf16[128,8,2048]{2,1,0:T(8,128)(2,1)}, u32[]{:S(2)}, u32[]{:S(2)}) async-start(bf16[128,8,2048]{2,1,0:T(8,128)(2,1)} %convert_bitcast_fusion), calls=%async_computation.1 | async-start | bytes 8388608 | tf_op jit(solution)/shard_map/all_to_all | solution.py:90
  90.2 0.0 copy-done.3
  90.2 0.1 copy.8.ids_ref
  90.3 0.0 copy-done.4
  90.4 0.1 copy.9.gates_ref
  90.5 52.4 %all-to-all-done.1 = bf16[128,8,2048]{2,1,0:T(8,128)(2,1)} async-done(((bf16[128,8,2048]{2,1,0:T(8,128)(2,1)}), bf16[128,8,2048]{2,1,0:T(8,128)(2,1)}, u32[]{:S(2)}, u32[]{:S(2)}) %all-to-all-start.1) | async-done | bytes 4194336 | tf_op jit(solution)/shard_map/all_to_all | solution.py:90
  142.9 5.9 %combine.1 = bf16[256,2048]{1,0:T(8,128)(2,1)} custom-call(bf16[1024,2048]{1,0:T(8,128)(2,1)} %bitcast.8.results_ref, s32[256,2]{1,0:T(8,128)S(1)} %copy.8.ids_ref, f32[256,2]{1,0:T(8,128)S(1)} %copy.9.gates_ref), custom_call_target="tpu_custom_call" | custom-call | tf_op jit(solution)/shard_map/combine/pallas_call | solution.py:91
  (2 shorter events, 0.0 us)
Async XLA Ops:
  0.0 1.2 copy-start
  1.2 0.7 copy-start.1
  1.9 0.7 copy-start.2
  4.3 64.2 %copy-start.5 = (bf16[1,2048,1024]{2,1,0:T(8,128)(2,1)S(1)}, bf16[1,2048,1024]{2,1,0:T(8,128)(2,1)}, u32[]{:S(2)}) copy-start(bf16[1,2048,1024]{2,1,0:T(8,128)(2,1)} %param.12) | copy-start | bytes 12582916
  68.6 4.5 %copy-start.6 = (bf16[1,2048,1024]{2,1,0:T(8,128)(2,1)S(1)}, bf16[1,2048,1024]{2,1,0:T(8,128)(2,1)}, u32[]{:S(2)}) copy-start(bf16[1,2048,1024]{2,1,0:T(8,128)(2,1)} %param.11) | copy-start | bytes 12582916
  73.1 5.4 %copy-start.7 = (bf16[1,1024,2048]{2,1,0:T(8,128)(2,1)S(1)}, bf16[1,1024,2048]{2,1,0:T(8,128)(2,1)}, u32[]{:S(2)}) copy-start(bf16[1,1024,2048]{2,1,0:T(8,128)(2,1)} %param.13) | copy-start | bytes 12582916
  84.5 5.7 %copy-start.3 = (s32[256,2]{0,1:T(2,128)S(1)}, s32[256,2]{0,1:T(2,128)}, u32[]{:S(2)}) copy-start(s32[256,2]{0,1:T(2,128)} %param.9) | copy-start | bytes 6148
  84.5 5.8 %copy-start.4 = (f32[256,2]{0,1:T(2,128)S(1)}, f32[256,2]{0,1:T(2,128)}, u32[]{:S(2)}) copy-start(f32[256,2]{0,1:T(2,128)} %param.10) | copy-start | bytes 6148
  84.5 58.4 %all-to-all-start.1 = ((bf16[128,8,2048]{2,1,0:T(8,128)(2,1)}), bf16[128,8,2048]{2,1,0:T(8,128)(2,1)}, u32[]{:S(2)}, u32[]{:S(2)}) async-start(bf16[128,8,2048]{2,1,0:T(8,128)(2,1)} %convert_bitcast_fusion), calls=%async_computation.1 | async-start | bytes 8388608 | tf_op jit(solution)/shard_map/all_to_all | solution.py:90

commit v2 on v1

v2 whole, which is shorter than its diff:
```python
import jax
import jax.numpy as jnp
from jax import lax
from jax.experimental import pallas as pl
from jax.experimental.pallas import tpu as pltpu
from jax.sharding import PartitionSpec as P

EPS = 1e-06
F32 = jnp.float32
BF16 = jnp.bfloat16
MESH = pl.DeviceIdType.MESH
SLOTS = 8
GROUP_SLOTS = 16
BATCHES = 4
RANKS = 8


def iota(shape, dim):
    return lax.broadcasted_iota(jnp.int32, shape, dim)


def ones_where(mask):
    return jnp.where(mask, 1.0, 0.0).astype(BF16)


def dot(a, b):
    return jnp.dot(a, b, preferred_element_type=F32)


def peer(me, batch, core, rank):
    dy = rank & 3
    x = ((me >> 1) & 3) ^ (3 * (rank >> 2))
    y = (((me >> 3) & 3) + dy) & 3
    z = ((me >> 5) + batch - dy) & 3
    return (z << 5) | (y << 3) | (x << 1) | ((me & 1) ^ core)


def expert_slots(ids_ref):
    rows = ids_ref.shape[1]
    first, second = ids_ref[0:1, :], ids_ref[1:2, :]
    expert = iota((128, rows), 0)
    is_first, is_second = expert == first, expert == second
    before = ones_where(iota((rows, rows), 0) < iota((rows, rows), 1))
    rank = dot(ones_where(is_first | is_second), before)
    slot_first = jnp.sum(jnp.where(is_first, rank, 0.0), axis=0, keepdims=True).astype(jnp.int32)
    slot_second = jnp.sum(jnp.where(is_second, rank, 0.0), axis=0, keepdims=True).astype(jnp.int32)
    return first, second, slot_first, slot_second


def pack(me, tokens_ref, gain_ref, ids_ref, out_ref, normed_ref):
    rows, width = tokens_ref.shape
    floats = tokens_ref[...].astype(F32)
    mean = jnp.sum(floats * floats, axis=1, keepdims=True) * (1.0 / width)
    normed_ref[...] = (floats * lax.rsqrt(mean + EPS) * gain_ref[...]).astype(BF16)
    first, second, slot_first, slot_second = expert_slots(ids_ref)
    count = BATCHES * 2 * RANKS * SLOTS
    row = iota((count, rows), 0)
    wanted = peer(me, row >> 7, (row >> 6) & 1, (row >> 3) & 7) * SLOTS + (row & 7)
    chosen = ones_where((wanted == first * SLOTS + slot_first) | (wanted == second * SLOTS + slot_second))
    for start in range(0, width, 512):
        columns = pl.ds(start, 512)
        block = dot(chosen, normed_ref[:, columns]).astype(BF16)
        out_ref[:, :, columns] = block.reshape(count // SLOTS, SLOTS, 512)


def describe(me, ids_ref, gates_ref, places_ref, meta_ref):
    rows = ids_ref.shape[1]
    first, second, slot_first, slot_second = expert_slots(ids_ref)
    group = first >> 2
    in_group = iota((32, rows), 0) == group
    before = ones_where(iota((rows, rows), 0) < iota((rows, rows), 1))
    rank = dot(ones_where(in_group), before)
    place = jnp.sum(jnp.where(in_group, rank, 0.0), axis=0, keepdims=True).astype(jnp.int32)
    side = ((me >> 1) ^ (me >> 2)) & 1
    relay = (((group & 1) ^ side) << 1) | (me & 1)
    source_first = ((first ^ relay) & 3) * 64 + slot_first
    source_second = ((second ^ relay) & 3) * 64 + slot_second
    count = BATCHES * RANKS * GROUP_SLOTS
    row = iota((count, rows), 0)
    wanted = (peer(me, row >> 7, 0, (row >> 4) & 7) >> 2) * GROUP_SLOTS + (row & 15)
    places = ones_where(wanted == group * GROUP_SLOTS + place)
    places_ref[...] = places
    values = [source_first.astype(F32), source_second.astype(F32)]
    for k in range(2):
        rest = gates_ref[k : k + 1, :]
        for _ in range(3):
            part = rest.astype(BF16).astype(F32)
            values.append(part)
            rest = rest - part
    kind = iota((128, rows), 0)
    table = jnp.zeros((128, rows), F32)
    for k, value in enumerate(values):
        table = jnp.where(kind == k, value, table)
    meta = lax.dot_general(places, table.astype(BF16), (((1,), (1,)), ((), ())), preferred_element_type=F32)
    meta_ref[...] = meta.astype(BF16).reshape(BATCHES * RANKS, GROUP_SLOTS, 128)


def layer_kernel(
    tokens_ref, gain_ref, ids_ref, gates_ref, w_gate_ref, w_up_ref, w_down_ref, out_ref,
    gate_w, up_w, down_w, near_tokens, near_ids, normed, packed, arrived, hidden, produced, gathered, places,
    meta_out, meta_in, sums, returned,
    weight_sem, raw_send, raw_recv, ids_send, ids_recv, meta_send, meta_recv, packed_send, arrived_recv,
    core_send, core_recv, cross_send, cross_recv, sums_send, returned_recv,
):
    me = lax.axis_index("ep")
    width = tokens_ref.shape[1]
    ff = hidden.shape[1]
    per_wave = BATCHES * 2 * RANKS

    def at(i):
        return peer(me, i >> 4, (i >> 3) & 1, i & 7)

    barrier = pltpu.get_barrier_semaphore()

    def greet(i, carry):
        pl.semaphore_signal(barrier, inc=1, device_id=(at(i),), device_id_type=MESH)
        return carry

    lax.fori_loop(1, per_wave, greet, 0)
    pl.semaphore_signal(barrier, inc=1, device_id=(me ^ 2,), device_id_type=MESH)
    pl.semaphore_signal(barrier, inc=1, device_id=(me ^ 3,), device_id_type=MESH)

    weights = [
        pltpu.make_async_copy(w_gate_ref.at[0], gate_w, weight_sem.at[0]),
        pltpu.make_async_copy(w_up_ref.at[0], up_w, weight_sem.at[1]),
        pltpu.make_async_copy(w_down_ref.at[0], down_w, weight_sem.at[2]),
    ]
    for copy in weights:
        copy.start()

    pl.semaphore_wait(barrier, per_wave + 1)

    raw = pltpu.make_async_remote_copy(
        tokens_ref, near_tokens, raw_send, raw_recv, device_id=(me ^ 2,), device_id_type=MESH
    )
    raw_ids = pltpu.make_async_remote_copy(
        ids_ref, near_ids, ids_send, ids_recv, device_id=(me ^ 2,), device_id_type=MESH
    )
    raw_ids.start()
    raw.start()

    def send_packed(wave):
        def send(i, carry):
            unit = wave * BATCHES + (i >> 4)
            pltpu.make_async_remote_copy(
                packed.at[wave, i], arrived.at[unit, i & 15], packed_send.at[wave], arrived_recv.at[unit],
                device_id=(at(i),), device_id_type=MESH,
            ).start()
            return carry

        lax.fori_loop(1, per_wave, send, 0)
        arrived[wave * BATCHES, 0] = packed[wave, 0]

    pack(me, tokens_ref, gain_ref, ids_ref, packed.at[0], normed)
    send_packed(0)
    describe(me, ids_ref, gates_ref, places, meta_out)

    def send_meta(i, carry):
        pltpu.make_async_remote_copy(
            meta_out.at[i], meta_in.at[i], meta_send, meta_recv,
            device_id=(peer(me, i >> 3, 0, i & 7),), device_id_type=MESH,
        ).start()
        return carry

    lax.fori_loop(1, BATCHES * RANKS, send_meta, 0)
    meta_in[0] = meta_out[0]

    for copy in weights:
        copy.wait()

    def expert(unit, carry):
        batch = unit & 3

        @pl.when(batch == 0)
        def _():
            view = arrived.at[unit, pl.ds(1, 15)]
            pltpu.make_async_copy(view, view, arrived_recv.at[unit]).wait()

        @pl.when(batch != 0)
        def _():
            view = arrived.at[unit]
            pltpu.make_async_copy(view, view, arrived_recv.at[unit]).wait()

        rows = arrived[unit].reshape(2 * RANKS * SLOTS, width)
        for start in range(0, ff, 256):
            columns = pl.ds(start, 256)
            gate_part = dot(rows, gate_w[:, columns])
            up_part = dot(rows, up_w[:, columns])
            hidden[:, columns] = (gate_part / (1.0 + jnp.exp(-gate_part)) * up_part).astype(BF16)
        for start in range(0, width, 256):
            columns = pl.ds(start, 256)
            block = dot(hidden[...], down_w[:, columns]).astype(BF16)
            produced[unit, :, :, columns] = block.reshape(2 * RANKS, SLOTS, 256)

        @pl.when(unit < BATCHES)
        def _():
            pltpu.make_async_remote_copy(
                produced.at[unit, pl.ds(RANKS, RANKS)], gathered.at[batch, 1], core_send, core_recv.at[batch],
                device_id=(me ^ 1,), device_id_type=MESH,
            ).start()
            gathered[batch, 0] = produced[unit, 0:RANKS]

        @pl.when(unit >= BATCHES)
        def _():
            for core in range(2):
                pltpu.make_async_remote_copy(
                    produced.at[unit, pl.ds(core * RANKS, RANKS)], gathered.at[batch, 2 + core],
                    cross_send.at[core], cross_recv.at[batch, core],
                    device_id=(me ^ (2 + core),), device_id_type=MESH,
                ).start()

        @pl.when(unit == 2)
        def _():
            raw_ids.wait_recv()
            raw.wait_recv()
            pack(me, near_tokens, gain_ref, near_ids, packed.at[1], normed)
            send_packed(1)

        @pl.when(unit == 6)
        def _():
            view = meta_in.at[pl.ds(1, BATCHES * RANKS - 1)]
            pltpu.make_async_copy(view, view, meta_recv).wait()

        @pl.when(unit >= 6)
        def _():
            relay(unit - 6)

        return carry

    def relay(batch):
        view = gathered.at[batch, 1]
        pltpu.make_async_copy(view, view, core_recv.at[batch]).wait()
        for core in range(2):
            view = gathered.at[batch, 2 + core]
            pltpu.make_async_copy(view, view, cross_recv.at[batch, core]).wait()
        count = RANKS * GROUP_SLOTS
        meta = meta_in[pl.ds(batch * RANKS, RANKS)].reshape(count, 128).astype(F32)
        base = (iota((count, 1), 0) // GROUP_SLOTS) * SLOTS
        column = iota((count, 4 * RANKS * SLOTS), 1)
        picks = [ones_where(column == meta[:, k : k + 1].astype(jnp.int32) + base) for k in range(2)]
        scale = [meta[:, 2 + 3 * k : 3 + 3 * k] + meta[:, 3 + 3 * k : 4 + 3 * k] + meta[:, 4 + 3 * k : 5 + 3 * k] for k in range(2)]
        for start in range(0, width, 512):
            columns = pl.ds(start, 512)
            rows = gathered[batch, :, :, :, columns].reshape(4 * RANKS * SLOTS, 512)
            total = dot(picks[0], rows) * scale[0] + dot(picks[1], rows) * scale[1]
            sums[batch, :, :, columns] = total.astype(BF16).reshape(RANKS, GROUP_SLOTS, 512)

        def send(rank, carry):
            pltpu.make_async_remote_copy(
                sums.at[batch, rank], returned.at[batch, rank], sums_send.at[batch], returned_recv.at[batch],
                device_id=(back(batch, rank),), device_id_type=MESH,
            ).start()
            return carry

        @pl.when(batch == 0)
        def _():
            returned[0, 0] = sums[0, 0]
            lax.fori_loop(1, RANKS, send, 0)

        @pl.when(batch != 0)
        def _():
            lax.fori_loop(0, RANKS, send, 0)

    def back(batch, rank):
        dy = rank & 3
        x = ((me >> 1) & 3) ^ (3 * (rank >> 2))
        y = (((me >> 3) & 3) - dy) & 3
        z = ((me >> 5) - batch + dy) & 3
        return (z << 5) | (y << 3) | (x << 1) | (me & 1)

    lax.fori_loop(0, 2 * BATCHES, expert, 0)

    def relay_step(batch, carry):
        relay(batch)
        return carry

    lax.fori_loop(2, BATCHES, relay_step, 0)

    for batch in range(BATCHES):
        view = returned.at[batch, pl.ds(1, RANKS - 1)] if batch == 0 else returned.at[batch]
        pltpu.make_async_copy(view, view, returned_recv.at[batch]).wait()
    chosen = places[...]
    for start in range(0, width, 512):
        columns = pl.ds(start, 512)
        rows = returned[:, :, :, columns].reshape(BATCHES * RANKS * GROUP_SLOTS, 512)
        block = lax.dot_general(chosen, rows, (((0,), (0,)), ((), ())), preferred_element_type=F32)
        out_ref[:, columns] = block.astype(BF16)

    raw.wait_send()
    raw_ids.wait_send()

    def drain(view, sem):
        pltpu.make_async_copy(view, view, sem).wait()

    for wave in range(2):
        drain(packed.at[wave, pl.ds(1, per_wave - 1)], packed_send.at[wave])
    drain(meta_out.at[pl.ds(1, BATCHES * RANKS - 1)], meta_send)
    drain(gathered.at[:, 1], core_send)
    for core in range(2):
        drain(gathered.at[:, 2 + core], cross_send.at[core])
    for batch in range(BATCHES):
        drain(sums.at[batch, pl.ds(1, RANKS - 1)] if batch == 0 else sums.at[batch], sums_send.at[batch])


def whole():
    return pl.BlockSpec(memory_space=pltpu.VMEM)


def shards(tokens, norm_gain, expert_ids, gates, w_gate, w_up, w_down):
    rows, width = tokens.shape
    ff = w_gate.shape[2]
    dma = pltpu.SemaphoreType.DMA
    return pl.pallas_call(
        layer_kernel,
        out_shape=jax.ShapeDtypeStruct((rows, width), BF16),
        in_specs=[whole()] * 4 + [pl.BlockSpec(memory_space=pl.ANY)] * 3,
        out_specs=whole(),
        scratch_shapes=[
            pltpu.VMEM((width, ff), BF16),
            pltpu.VMEM((width, ff), BF16),
            pltpu.VMEM((ff, width), BF16),
            pltpu.VMEM((rows, width), BF16),
            pltpu.VMEM((2, rows), jnp.int32),
            pltpu.VMEM((rows, width), BF16),
            pltpu.VMEM((2, BATCHES * 2 * RANKS, SLOTS, width), BF16),
            pltpu.VMEM((2 * BATCHES, 2 * RANKS, SLOTS, width), BF16),
            pltpu.VMEM((2 * RANKS * SLOTS, ff), BF16),
            pltpu.VMEM((2 * BATCHES, 2 * RANKS, SLOTS, width), BF16),
            pltpu.VMEM((BATCHES, 4, RANKS, SLOTS, width), BF16),
            pltpu.VMEM((BATCHES * RANKS * GROUP_SLOTS, rows), BF16),
            pltpu.VMEM((BATCHES * RANKS, GROUP_SLOTS, 128), BF16),
            pltpu.VMEM((BATCHES * RANKS, GROUP_SLOTS, 128), BF16),
            pltpu.VMEM((BATCHES, RANKS, GROUP_SLOTS, width), BF16),
            pltpu.VMEM((BATCHES, RANKS, GROUP_SLOTS, width), BF16),
            dma((3,)), dma, dma, dma, dma, dma, dma, dma((2,)), dma((2 * BATCHES,)),
            dma, dma((BATCHES,)), dma((2,)), dma((BATCHES, 2)), dma((BATCHES,)), dma((BATCHES,)),
        ],
        compiler_params=pltpu.CompilerParams(
            collective_id=0, has_side_effects=True, vmem_limit_bytes=60 << 20
        ),
        name="layer",
    )(tokens, norm_gain.reshape(1, width), expert_ids.T, gates.T, w_gate, w_up, w_down)


def solution(mesh):
    return jax.shard_map(
        shards,
        mesh=mesh,
        in_specs=(
            P("ep", None),
            P(),
            P("ep", None),
            P("ep", None),
            P("ep", None, None),
            P("ep", None, None),
            P("ep", None, None),
        ),
        out_specs=P("ep", None),
        check_vma=False,
    )
```

time: 149 us -> 113 us (0.76); the launches traced: 149 us -> 111 us
  Pallas kernels: 7.64 us -> 108 us
  blocking collectives: 64.2 us -> 0 us
  waiting for transfers between devices: 52.4 us -> 0 us
  matrix products: 15.9 us -> 0 us
  starting transfers between devices: 5.65 us -> 0 us
    pallas_call x2 -> x1, Pallas kernels: 7.64 us -> 108 us  [shards(): pl.pallas_call(layer_kernel, out_shape=jax.ShapeDtypeStruct((rows, width)...]
    all_to_all x1 -> x0, blocking collectives: 64.2 us -> none  [shards(): lax.all_to_all(outgoing.reshape(experts, 8, width), 'ep', split_axis=0, c...]
    all_to_all x1 -> x0, waiting for transfers between devices: 52.4 us -> none  [shards(): lax.all_to_all(produced.reshape(experts, 8, width), 'ep', split_axis=0, c...]
    dot_general x3 -> x0, matrix products: 15.9 us -> none  [dot(): return jnp.dot(a, b, preferred_element_type=F32)]
    all_to_all x1 -> x0, starting transfers between devices: 5.65 us -> none  [shards(): lax.all_to_all(produced.reshape(experts, 8, width), 'ep', split_axis=0, c...]
  transfers between devices with their start and end apart: 1 -> 0, of which waited for: 1 -> 0; matrix products, arithmetic and copies ran while one was open for 0% -> 0% of each run, Pallas kernels for 0% -> 0%
where the time goes in v2:
time: 113 us; the launch traced here: 111 us
  Pallas kernels  108 us (96%)
  local copies, waits for them, and re-layouts  2.3 us (2%)
    pallas_call x1, Pallas kernels, shards(): pl.pallas_call(layer_kernel, out_shape=jax.ShapeDtypeStruct((rows, width)...  108 us
    unnamed x1, local copies, waits for them, and re-layouts  2.3 us

profile of v2, /device:TPU:1, one launch (start us, length us, event | category | flops | bytes accessed | tf_op | source)
XLA Modules:
  0.0 110.7 jit_solution(11931616609599598276)
XLA Ops:
  0.0 108.4 %layer.1 = bf16[256,2048]{1,0:T(8,128)(2,1)} custom-call(bf16[256,2048]{1,0:T(8,128)(2,1)} %tokens_ref.1, f32[1,2048]{1,0:T(1,128)} %bitcast.3, s32[2,256]{1,0:T(2,128)} %bitcast.4, f32[2,256]{1,0:T(2,128)} %bitcast.5, bf16[1,2048,1024]{2,1,0:T(8,128)(2,1)} %w_gate_ref.1, bf16[1,2048,1024]{2,1,0:T(8,128)(2,1)} %w_up_ref.1, bf16[1,1024,2048]{2,1,0:T(8,128)(2,1)} %w_down_ref.1), custom_call_target="tpu_custom_call" | custom-call | tf_op jit(solution)/shard_map/layer/pallas_call | solution.py:313
  108.4 2.3 %copy.9 = bf16[256,2048]{1,0:T(8,128)(2,1)} copy(bf16[256,2048]{1,0:T(8,128)(2,1)} %layer.1) | data formatting | bytes 2097152

commit v3 on v2

v3 whole, which is shorter than its diff:
```python
import jax
import jax.numpy as jnp
from jax import lax
from jax.experimental import pallas as pl
from jax.experimental.pallas import tpu as pltpu
from jax.sharding import PartitionSpec as P

EPS = 1e-06
F32 = jnp.float32
BF16 = jnp.bfloat16
MESH = pl.DeviceIdType.MESH
SLOTS = 8
GROUP_SLOTS = 16
BATCHES = 4
RANKS = 8


def iota(shape, dim):
    return lax.broadcasted_iota(jnp.int32, shape, dim)


def ones_where(mask):
    return jnp.where(mask, 1.0, 0.0).astype(BF16)


def dot(a, b):
    return jnp.dot(a, b, preferred_element_type=F32)


def turns(batch):
    return batch ^ (batch >> 1)


def peer(me, batch, core, rank):
    dy = rank & 3
    x = ((me >> 1) & 3) ^ (3 * (rank >> 2))
    y = (((me >> 3) & 3) + dy) & 3
    z = ((me >> 5) + turns(batch) - dy) & 3
    return (z << 5) | (y << 3) | (x << 1) | ((me & 1) ^ core)


def expert_slots(ids_ref):
    rows = ids_ref.shape[1]
    first, second = ids_ref[0:1, :], ids_ref[1:2, :]
    expert = iota((128, rows), 0)
    is_first, is_second = expert == first, expert == second
    before = ones_where(iota((rows, rows), 0) < iota((rows, rows), 1))
    rank = dot(ones_where(is_first | is_second), before)
    slot_first = jnp.sum(jnp.where(is_first, rank, 0.0), axis=0, keepdims=True).astype(jnp.int32)
    slot_second = jnp.sum(jnp.where(is_second, rank, 0.0), axis=0, keepdims=True).astype(jnp.int32)
    return first, second, slot_first, slot_second


def normalize(tokens_ref, gain_ref, normed_ref, start, count):
    rows = pl.ds(start, count)
    floats = tokens_ref[rows, :].astype(F32)
    mean = jnp.sum(floats * floats, axis=1, keepdims=True) * (1.0 / floats.shape[1])
    normed_ref[rows, :] = (floats * lax.rsqrt(mean + EPS) * gain_ref[...]).astype(BF16)


def choose(me, ids_ref, chosen_ref):
    count, rows = chosen_ref.shape
    first, second, slot_first, slot_second = expert_slots(ids_ref)
    row = iota((count, rows), 0)
    wanted = peer(me, row >> 7, (row >> 6) & 1, (row >> 3) & 7) * SLOTS + (row & 7)
    chosen_ref[...] = ones_where((wanted == first * SLOTS + slot_first) | (wanted == second * SLOTS + slot_second))


def lay_out(chosen_ref, normed_ref, out_ref, half):
    blocks = out_ref.shape[0] // 2
    rows = pl.ds(half * blocks * SLOTS, blocks * SLOTS)
    for start in range(0, normed_ref.shape[1], 512):
        columns = pl.ds(start, 512)
        block = dot(chosen_ref[rows, :], normed_ref[:, columns]).astype(BF16)
        out_ref[pl.ds(half * blocks, blocks), :, columns] = block.reshape(blocks, SLOTS, 512)


def describe(me, ids_ref, gates_ref, places_ref, meta_ref):
    rows = ids_ref.shape[1]
    first, second, slot_first, slot_second = expert_slots(ids_ref)
    group = first >> 2
    in_group = iota((32, rows), 0) == group
    before = ones_where(iota((rows, rows), 0) < iota((rows, rows), 1))
    rank = dot(ones_where(in_group), before)
    place = jnp.sum(jnp.where(in_group, rank, 0.0), axis=0, keepdims=True).astype(jnp.int32)
    side = ((me >> 1) ^ (me >> 2)) & 1
    relay = (((group & 1) ^ side) << 1) | (me & 1)
    source_first = ((first ^ relay) & 3) * 64 + slot_first
    source_second = ((second ^ relay) & 3) * 64 + slot_second
    count = BATCHES * RANKS * GROUP_SLOTS
    row = iota((count, rows), 0)
    wanted = (peer(me, row >> 7, 0, (row >> 4) & 7) >> 2) * GROUP_SLOTS + (row & 15)
    places = ones_where(wanted == group * GROUP_SLOTS + place)
    places_ref[...] = places
    values = [source_first.astype(F32), source_second.astype(F32)]
    for k in range(2):
        rest = gates_ref[k : k + 1, :]
        for _ in range(3):
            part = rest.astype(BF16).astype(F32)
            values.append(part)
            rest = rest - part
    kind = iota((128, rows), 0)
    table = jnp.zeros((128, rows), F32)
    for k, value in enumerate(values):
        table = jnp.where(kind == k, value, table)
    meta = lax.dot_general(places, table.astype(BF16), (((1,), (1,)), ((), ())), preferred_element_type=F32)
    meta_ref[...] = meta.astype(BF16).reshape(BATCHES * RANKS, GROUP_SLOTS, 128)


def layer_kernel(
    tokens_ref, gain_hbm, ids_hbm, gates_hbm, w_gate_ref, w_up_ref, w_down_ref, out_ref,
    gate_w, up_w, down_w, gain_ref, ids_ref, gates_ref, own_tokens, near_tokens, near_ids, normed, chosen, packed,
    arrived, hidden, produced, gathered, places, meta_out, meta_in, sums, returned,
    weight_sem, load_sem, turn_sem, raw_send, raw_recv, ids_send, ids_recv, meta_send, meta_recv,
    packed_send, arrived_recv, core_send, core_recv, cross_send, cross_recv, sums_send, returned_recv,
):
    me = lax.axis_index("ep")
    core = me & 1
    rows, width = own_tokens.shape
    ff = hidden.shape[1]
    per_wave = BATCHES * 2 * RANKS

    barrier = pltpu.get_barrier_semaphore()

    def greet(device):
        pl.semaphore_signal(barrier, inc=1, device_id=(device,), device_id_type=MESH)

    def greet_plane(i, carry):
        plane = ((me + (i << 5)) & 96) | ((me + ((i >> 2) << 3)) & 24)
        for flip in (7, 6, 1):
            greet(plane | ((me & 7) ^ flip))

        @pl.when(i != 0)
        def _():
            greet(plane | (me & 7))

        return carry

    lax.fori_loop(0, 16, greet_plane, 0)
    greet(me ^ 2)
    greet(me ^ 3)

    loads = [
        pltpu.make_async_copy(ids_hbm, ids_ref, load_sem.at[0]),
        pltpu.make_async_copy(tokens_ref, own_tokens, load_sem.at[1]),
        pltpu.make_async_copy(gain_hbm, gain_ref, load_sem.at[2]),
        pltpu.make_async_copy(gates_hbm, gates_ref, load_sem.at[3]),
    ]
    weights = [
        pltpu.make_async_copy(w_gate_ref.at[0], gate_w, weight_sem.at[0]),
        pltpu.make_async_copy(w_up_ref.at[0], up_w, weight_sem.at[1]),
        pltpu.make_async_copy(w_down_ref.at[0], down_w, weight_sem.at[2]),
    ]
    for copy in loads:
        copy.start()

    chunks = [(0, 3 * rows // 8), (3 * rows // 8, 3 * rows // 8), (3 * rows // 4, rows // 8), (7 * rows // 8, rows // 8)]
    raw = [
        pltpu.make_async_remote_copy(
            tokens_ref.at[pl.ds(start, count)], near_tokens.at[pl.ds(start, count)], raw_send.at[k], raw_recv.at[k],
            device_id=(me ^ 2,), device_id_type=MESH,
        )
        for k, (start, count) in enumerate(chunks)
    ]
    raw_ids = pltpu.make_async_remote_copy(
        ids_hbm, near_ids, ids_send, ids_recv, device_id=(me ^ 2,), device_id_type=MESH
    )

    def send_packed(wave, half):
        first_unit = BATCHES * (3 * core if wave == 0 else 1 + core)
        blocks = per_wave // 2

        def send(i, carry):
            batch, rank = i >> 4, i & 7
            pltpu.make_async_remote_copy(
                packed.at[wave, i], arrived.at[first_unit + batch, rank],
                packed_send.at[wave], arrived_recv.at[first_unit + batch],
                device_id=(peer(me, batch, (i >> 3) & 1, rank),), device_id_type=MESH,
            ).start()
            return carry

        lax.fori_loop(max(1, half * blocks), (half + 1) * blocks, send, 0)
        if half == 0:
            arrived[first_unit, 0] = packed[wave, 0]

    def wait_barrier():
        with jax.named_scope("barrier"):
            pl.semaphore_wait(barrier, per_wave + 1)

    wait_barrier()
    raw_ids.start()

    @pl.when(core == 0)
    def _():
        for copy in raw:
            copy.start()

    for copy in loads:
        copy.wait()
    for copy in weights:
        copy.start()
    with jax.named_scope("pack_own"):
        choose(me, ids_ref, chosen)
        normalize(own_tokens, gain_ref, normed, 0, rows)
        for half in range(2):
            lay_out(chosen, normed, packed.at[0], half)

            @pl.when(core == 0)
            def _():
                send_packed(0, half)

    with jax.named_scope("describe"):
        describe(me, ids_ref, gates_ref, places, meta_out)

    def send_meta(i, carry):
        pltpu.make_async_remote_copy(
            meta_out.at[i], meta_in.at[i], meta_send, meta_recv,
            device_id=(peer(me, i >> 3, 0, i & 7),), device_id_type=MESH,
        ).start()
        return carry

    lax.fori_loop(1, BATCHES * RANKS, send_meta, 0)
    meta_in[0] = meta_out[0]
    with jax.named_scope("ids_wait"):
        raw_ids.wait_recv()
        choose(me, near_ids, chosen)

    @pl.when(core == 1)
    def _():
        with jax.named_scope("turn"):
            pl.semaphore_wait(turn_sem, 1)
        for copy in raw:
            copy.start()

    def near():
        for k, (start, count) in enumerate(chunks):
            with jax.named_scope("raw_wait"):
                raw[k].wait_recv()

            if k == 2:
                @pl.when(core == 0)
                def _():
                    pl.semaphore_signal(turn_sem, inc=1, device_id=(me ^ 1,), device_id_type=MESH)

            normalize(near_tokens, gain_ref, normed, start, count)
        with jax.named_scope("pack_near"):
            lay_out(chosen, normed, packed.at[1], 0)
            send_packed(1, 0)
            lay_out(chosen, normed, packed.at[1], 1)
            send_packed(1, 1)

        @pl.when(core == 1)
        def _():
            send_packed(0, 0)
            send_packed(0, 1)

    def wait_unit(unit, batch, source_core):
        alone = (batch == 0) & (source_core == core)

        @pl.when(alone)
        def _():
            view = arrived.at[unit, pl.ds(1, RANKS - 1)]
            pltpu.make_async_copy(view, view, arrived_recv.at[unit]).wait()

        @pl.when(jnp.logical_not(alone))
        def _():
            view = arrived.at[unit]
            pltpu.make_async_copy(view, view, arrived_recv.at[unit]).wait()

    def expert(unit, carry):
        @pl.when(unit == 6 * core)
        def _():
            near()

        batch, kind = unit & 3, unit >> 2
        source_core = kind >> 1
        crossing = (kind == 1) | (kind == 2)
        with jax.named_scope("unit_wait"):
            wait_unit(unit, batch, source_core)

        @pl.when(unit == 0)
        def _():
            for copy in weights:
                copy.wait()

        with jax.named_scope("unit"):
            block_rows = arrived[unit].reshape(RANKS * SLOTS, width)
            for start in range(0, ff, 256):
                columns = pl.ds(start, 256)
                gate_part = dot(block_rows, gate_w[:, columns])
                up_part = dot(block_rows, up_w[:, columns])
                hidden[:, columns] = (gate_part / (1.0 + jnp.exp(-gate_part)) * up_part).astype(BF16)
            for start in range(0, width, 256):
                columns = pl.ds(start, 256)
                block = dot(hidden[...], down_w[:, columns]).astype(BF16)
                produced[unit, :, :, columns] = block.reshape(RANKS, SLOTS, 256)

        other = source_core ^ core

        @pl.when(crossing)
        def _():
            pltpu.make_async_remote_copy(
                produced.at[unit], gathered.at[batch, 2 + other],
                cross_send.at[source_core], cross_recv.at[batch, other],
                device_id=(me ^ (2 + other),), device_id_type=MESH,
            ).start()

        @pl.when(jnp.logical_not(crossing) & (other == 1))
        def _():
            pltpu.make_async_remote_copy(
                produced.at[unit], gathered.at[batch, 1], core_send, core_recv.at[batch],
                device_id=(me ^ 1,), device_id_type=MESH,
            ).start()

        @pl.when(jnp.logical_not(crossing) & (other == 0))
        def _():
            gathered[batch, 0] = produced[unit]

        @pl.when(((core == 0) & (unit >= 8) & (unit < 12)) | (core == 1) & (unit >= 12))
        def _():
            relay(batch)

        return carry

    def relay(batch):
        with jax.named_scope("relay_wait"):
            @pl.when(batch == 0)
            def _():
                view = meta_in.at[pl.ds(1, BATCHES * RANKS - 1)]
                pltpu.make_async_copy(view, view, meta_recv).wait()

            view = gathered.at[batch, 1]
            pltpu.make_async_copy(view, view, core_recv.at[batch]).wait()
            for other in range(2):
                view = gathered.at[batch, 2 + other]
                pltpu.make_async_copy(view, view, cross_recv.at[batch, other]).wait()
        count = RANKS * GROUP_SLOTS
        meta = meta_in[pl.ds(batch * RANKS, RANKS)].reshape(count, 128).astype(F32)
        base = (iota((count, 1), 0) // GROUP_SLOTS) * SLOTS
        column = iota((count, 4 * RANKS * SLOTS), 1)
        picks = [ones_where(column == meta[:, k : k + 1].astype(jnp.int32) + base) for k in range(2)]
        scale = [meta[:, k : k + 1] + meta[:, k + 1 : k + 2] + meta[:, k + 2 : k + 3] for k in (2, 5)]
        for start in range(0, width, 512):
            columns = pl.ds(start, 512)
            rows = gathered[batch, :, :, :, columns].reshape(4 * RANKS * SLOTS, 512)
            total = dot(picks[0], rows) * scale[0] + dot(picks[1], rows) * scale[1]
            sums[batch, :, :, columns] = total.astype(BF16).reshape(RANKS, GROUP_SLOTS, 512)

        def send(rank, carry):
            pltpu.make_async_remote_copy(
                sums.at[batch, rank], returned.at[batch, rank], sums_send.at[batch], returned_recv.at[batch],
                device_id=(back(batch, rank),), device_id_type=MESH,
            ).start()
            return carry

        @pl.when(batch == 0)
        def _():
            returned[0, 0] = sums[0, 0]
            lax.fori_loop(1, RANKS, send, 0)

        @pl.when(batch != 0)
        def _():
            lax.fori_loop(0, RANKS, send, 0)

    def back(batch, rank):
        dy = rank & 3
        x = ((me >> 1) & 3) ^ (3 * (rank >> 2))
        y = (((me >> 3) & 3) - dy) & 3
        z = ((me >> 5) - turns(batch) + dy) & 3
        return (z << 5) | (y << 3) | (x << 1) | (me & 1)

    lax.fori_loop(0, 4 * BATCHES, expert, 0)

    with jax.named_scope("return_wait"):
        for batch in range(BATCHES):
            view = returned.at[batch, pl.ds(1, RANKS - 1)] if batch == 0 else returned.at[batch]
            pltpu.make_async_copy(view, view, returned_recv.at[batch]).wait()
    chosen = places[...]
    for start in range(0, width, 512):
        columns = pl.ds(start, 512)
        rows = returned[:, :, :, columns].reshape(BATCHES * RANKS * GROUP_SLOTS, 512)
        block = lax.dot_general(chosen, rows, (((0,), (0,)), ((), ())), preferred_element_type=F32)
        out_ref[:, columns] = block.astype(BF16)

    for copy in raw:
        copy.wait_send()
    raw_ids.wait_send()

    def drain(view, sem):
        pltpu.make_async_copy(view, view, sem).wait()

    for wave in range(2):
        drain(packed.at[wave, pl.ds(1, per_wave - 1)], packed_send.at[wave])
    drain(meta_out.at[pl.ds(1, BATCHES * RANKS - 1)], meta_send)
    drain(gathered.at[:, 1], core_send)
    for source_core in range(2):
        drain(gathered.at[:, 2], cross_send.at[source_core])
    for batch in range(BATCHES):
        drain(sums.at[batch, pl.ds(1, RANKS - 1)] if batch == 0 else sums.at[batch], sums_send.at[batch])


def whole():
    return pl.BlockSpec(memory_space=pltpu.VMEM)


def shards(tokens, norm_gain, expert_ids, gates, w_gate, w_up, w_down):
    rows, width = tokens.shape
    ff = w_gate.shape[2]
    dma = pltpu.SemaphoreType.DMA
    return pl.pallas_call(
        layer_kernel,
        out_shape=jax.ShapeDtypeStruct((rows, width), BF16),
        in_specs=[pl.BlockSpec(memory_space=pltpu.HBM)] * 7,
        out_specs=whole(),
        scratch_shapes=[
            pltpu.VMEM((width, ff), BF16),
            pltpu.VMEM((width, ff), BF16),
            pltpu.VMEM((ff, width), BF16),
            pltpu.VMEM((1, width), F32),
            pltpu.VMEM((2, rows), jnp.int32),
            pltpu.VMEM((2, rows), F32),
            pltpu.VMEM((rows, width), BF16),
            pltpu.VMEM((rows, width), BF16),
            pltpu.VMEM((2, rows), jnp.int32),
            pltpu.VMEM((rows, width), BF16),
            pltpu.VMEM((BATCHES * 2 * RANKS * SLOTS, rows), BF16),
            pltpu.VMEM((2, BATCHES * 2 * RANKS, SLOTS, width), BF16),
            pltpu.VMEM((4 * BATCHES, RANKS, SLOTS, width), BF16),
            pltpu.VMEM((RANKS * SLOTS, ff), BF16),
            pltpu.VMEM((4 * BATCHES, RANKS, SLOTS, width), BF16),
            pltpu.VMEM((BATCHES, 4, RANKS, SLOTS, width), BF16),
            pltpu.VMEM((BATCHES * RANKS * GROUP_SLOTS, rows), BF16),
            pltpu.VMEM((BATCHES * RANKS, GROUP_SLOTS, 128), BF16),
            pltpu.VMEM((BATCHES * RANKS, GROUP_SLOTS, 128), BF16),
            pltpu.VMEM((BATCHES, RANKS, GROUP_SLOTS, width), BF16),
            pltpu.VMEM((BATCHES, RANKS, GROUP_SLOTS, width), BF16),
            dma((3,)), dma((4,)), pltpu.SemaphoreType.REGULAR, dma((4,)), dma((4,)), dma, dma, dma, dma,
            dma((2,)), dma((4 * BATCHES,)),
            dma, dma((BATCHES,)), dma((2,)), dma((BATCHES, 2)), dma((BATCHES,)), dma((BATCHES,)),
        ],
        compiler_params=pltpu.CompilerParams(
            collective_id=0, has_side_effects=True, vmem_limit_bytes=60 << 20
        ),
        name="layer",
    )(tokens, norm_gain.reshape(1, width), expert_ids.T, gates.T, w_gate, w_up, w_down)


def solution(mesh):
    return jax.shard_map(
        shards,
        mesh=mesh,
        in_specs=(
            P("ep", None),
            P(),
            P("ep", None),
            P("ep", None),
            P("ep", None, None),
            P("ep", None, None),
            P("ep", None, None),
        ),
        out_specs=P("ep", None),
        check_vma=False,
    )
```

time: 113 us -> 94.1 us (0.83); the launches traced: 111 us -> 94 us
  Pallas kernels: 108 us -> 91.7 us
    pallas_call x1, Pallas kernels: 108 us -> 91.7 us  [shards(): pl.pallas_call(layer_kernel, out_shape=jax.ShapeDtypeStruct((rows, width)...]
where the time goes in v3:
time: 94.1 us; the launch traced here: 94 us
  Pallas kernels  91.7 us (97%)
  local copies, waits for them, and re-layouts  2.3 us (2%)
    pallas_call x1, Pallas kernels, shards(): pl.pallas_call(layer_kernel, out_shape=jax.ShapeDtypeStruct((rows, width)...  91.7 us
    unnamed x1, local copies, waits for them, and re-layouts  2.3 us

profile of v3, /device:TPU:1, one launch (start us, length us, event | category | flops | bytes accessed | tf_op | source)
XLA Modules:
  0.0 94.0 jit_solution(3686005426452498926)
XLA Ops:
  0.0 91.7 %layer.1 = bf16[256,2048]{1,0:T(8,128)(2,1)} custom-call(bf16[256,2048]{1,0:T(8,128)(2,1)} %tokens_ref.1, f32[1,2048]{1,0:T(1,128)} %bitcast.3, s32[2,256]{1,0:T(2,128)} %bitcast.4, f32[2,256]{1,0:T(2,128)} %bitcast.5, bf16[1,2048,1024]{2,1,0:T(8,128)(2,1)} %w_gate_ref.1, bf16[1,2048,1024]{2,1,0:T(8,128)(2,1)} %w_up_ref.1, bf16[1,1024,2048]{2,1,0:T(8,128)(2,1)} %w_down_ref.1), custom_call_target="tpu_custom_call" | custom-call | tf_op jit(solution)/shard_map/layer/pallas_call | solution.py:410
  91.7 2.3 %copy.9 = bf16[256,2048]{1,0:T(8,128)(2,1)} copy(bf16[256,2048]{1,0:T(8,128)(2,1)} %layer.1) | data formatting | bytes 2097152

commit v4 on v3

--- a/solution.py
+++ b/solution.py
@@ -110,7 +110,7 @@
 def layer_kernel(
     tokens_ref, gain_hbm, ids_hbm, gates_hbm, w_gate_ref, w_up_ref, w_down_ref, out_ref,
     gate_w, up_w, down_w, gain_ref, ids_ref, gates_ref, own_tokens, near_tokens, near_ids, normed, chosen, packed,
-    arrived, hidden, produced, gathered, places, meta_out, meta_in, sums, returned,
+    arrived, hidden, produced, gathered, places, meta_out, meta_in, sums, returned, total,
     weight_sem, load_sem, turn_sem, raw_send, raw_recv, ids_send, ids_recv, meta_send, meta_recv,
     packed_send, arrived_recv, core_send, core_recv, cross_send, cross_recv, sums_send, returned_recv,
 ):
@@ -371,16 +371,28 @@
 
     lax.fori_loop(0, 4 * BATCHES, expert, 0)
 
-    with jax.named_scope("return_wait"):
-        for batch in range(BATCHES):
-            view = returned.at[batch, pl.ds(1, RANKS - 1)] if batch == 0 else returned.at[batch]
-            pltpu.make_async_copy(view, view, returned_recv.at[batch]).wait()
-    chosen = places[...]
+    def wait_returned(batch):
+        view = returned.at[batch, pl.ds(1, RANKS - 1)] if batch == 0 else returned.at[batch]
+        pltpu.make_async_copy(view, view, returned_recv.at[batch]).wait()
+
+    def bring(start, stop, columns):
+        count = RANKS * GROUP_SLOTS
+        back_rows = returned[start:stop, :, :, columns].reshape((stop - start) * count, 512)
+        return lax.dot_general(
+            places[start * count : stop * count], back_rows, (((0,), (0,)), ((), ())), preferred_element_type=F32
+        )
+
+    last = BATCHES - 1
+    for batch in range(last):
+        wait_returned(batch)
     for start in range(0, width, 512):
         columns = pl.ds(start, 512)
-        rows = returned[:, :, :, columns].reshape(BATCHES * RANKS * GROUP_SLOTS, 512)
-        block = lax.dot_general(chosen, rows, (((0,), (0,)), ((), ())), preferred_element_type=F32)
-        out_ref[:, columns] = block.astype(BF16)
+        total[:, columns] = bring(0, last, columns)
+    with jax.named_scope("return_wait"):
+        wait_returned(last)
+    for start in range(0, width, 512):
+        columns = pl.ds(start, 512)
+        out_ref[:, columns] = (total[:, columns] + bring(last, BATCHES, columns)).astype(BF16)
 
     for copy in raw:
         copy.wait_send()
@@ -434,6 +446,7 @@
             pltpu.VMEM((BATCHES * RANKS, GROUP_SLOTS, 128), BF16),
             pltpu.VMEM((BATCHES, RANKS, GROUP_SLOTS, width), BF16),
             pltpu.VMEM((BATCHES, RANKS, GROUP_SLOTS, width), BF16),
+            pltpu.VMEM((rows, width), F32),
             dma((3,)), dma((4,)), pltpu.SemaphoreType.REGULAR, dma((4,)), dma((4,)), dma, dma, dma, dma,
             dma((2,)), dma((4 * BATCHES,)),
             dma, dma((BATCHES,)), dma((2,)), dma((BATCHES, 2)), dma((BATCHES,)), dma((BATCHES,)),

time: 94.1 us -> 93.9 us (level)
  no operation moved by 1% of the time
where the time goes in v4:
time: 93.9 us; the launch traced here: 93.7 us
  Pallas kernels  91.4 us (97%)
  local copies, waits for them, and re-layouts  2.3 us (2%)
    pallas_call x1, Pallas kernels, shards(): pl.pallas_call(layer_kernel, out_shape=jax.ShapeDtypeStruct((rows, width)...  91.4 us
    unnamed x1, local copies, waits for them, and re-layouts  2.3 us

profile of v4, /device:TPU:1, one launch (start us, length us, event | category | flops | bytes accessed | tf_op | source)
XLA Modules:
  0.0 93.7 jit_solution(9349819088494367361)
XLA Ops:
  0.0 91.4 %layer.1 = bf16[256,2048]{1,0:T(8,128)(2,1)} custom-call(bf16[256,2048]{1,0:T(8,128)(2,1)} %tokens_ref.1, f32[1,2048]{1,0:T(1,128)} %bitcast.3, s32[2,256]{1,0:T(2,128)} %bitcast.4, f32[2,256]{1,0:T(2,128)} %bitcast.5, bf16[1,2048,1024]{2,1,0:T(8,128)(2,1)} %w_gate_ref.1, bf16[1,2048,1024]{2,1,0:T(8,128)(2,1)} %w_up_ref.1, bf16[1,1024,2048]{2,1,0:T(8,128)(2,1)} %w_down_ref.1), custom_call_target="tpu_custom_call" | custom-call | tf_op jit(solution)/shard_map/layer/pallas_call | solution.py:422
  91.4 2.3 %copy.9 = bf16[256,2048]{1,0:T(8,128)(2,1)} copy(bf16[256,2048]{1,0:T(8,128)(2,1)} %layer.1) | data formatting | bytes 2097152
